TPU v7x, 32 devices: a whole 2x2x4 slice. The times are simulated.
32 devices in a mesh: grp: 2 (over x), sp: 4 (over y, core), tp: 4 (over z).
Axes of the slice: x: 2, y: 2, z: 4, core: 2. Of those that a mesh axis runs over, the one named last changes fastest.
Arguments:
- residual: bfloat16 [768, 8, 2048], P(('sp', 'tp'), 'grp'), parts along dimension 1, may hold values from -6 to 6
- query: bfloat16 [768, 8, 1536], P('sp', 'grp', 'tp'), parts along dimension 1, may hold values from -64 to 64
- latent: bfloat16 [768, 8, 512], P('sp', 'grp'), parts along dimension 1, may hold values from -6 to 6
- rope_key: bfloat16 [768, 8, 64], P('sp', 'grp'), parts along dimension 1, may hold values from -8 to 8
- latent_gain: float32 [512], replicated, may hold values from 0.1 to 1.9
- key_up: bfloat16 [512, 1024], P(None, 'tp'), may hold values from -0.25 to 0.25
- value_up: bfloat16 [512, 1024], P(None, 'tp'), may hold values from -0.25 to 0.25
- out_weight: bfloat16 [1024, 2048], P('tp'), may hold values from -0.375 to 0.375
- norm_gain: float32 [2048], replicated, may hold values from 0.1 to 1.9
- group_prob: float32 [768, 8], P(('sp', 'tp'), 'grp'), parts along dimension 1, may hold values from 0.25 to 1
- pair_logits: float32 [768, 8, 2], P(('sp', 'tp'), 'grp'), parts along dimension 1, may hold values from -8 to 8
- routes: int32 [768, 8, 2], P(('sp', 'tp'), 'grp'), parts along dimension 1, may hold values from 0 to 15, all different within a row; in each aligned block of 192 rows (0 to 191, 192 to 383, ..., all dimensions but the last counted through in order) at most 36 rows name the same one
- w_gate: bfloat16 [16, 2048, 768], P(('sp', 'tp')), may hold values from -0.125 to 0.125
- w_up: bfloat16 [16, 2048, 768], P(('sp', 'tp')), may hold values from -0.125 to 0.125
- w_down: bfloat16 [16, 768, 2048], P(('sp', 'tp')), may hold values from -0.4375 to 0.4375
Outputs:
- layer_out: bfloat16 [768, 8, 2048], P(('sp', 'tp'), 'grp'), parts along dimension 1
There are 2 independent parts, one for each index of `grp`. A program takes and returns all parts, laid end to end along the dimension named above; an argument that names none is the same for every part. Nothing has to cross between parts.
Inputs may be any that keep to these rules, and one draw needn't show every extreme that they name: `routes`: A token's 2 experts differ. Among the tokens of one device (aligned blocks of 192 rows in position-then-sequence order), no expert is named more than 36 times, a bound that some block reaches.
All inputs are finite; a program needn't handle non-finite values.
Results may differ from a plain program's by a relative error of at most 0.013.
Values may be sent and summed in bfloat16 or wider, within the bound.
A program may use at most 128 MiB of HBM per device.

v0:
```python
import jax
import jax.numpy as jnp
from jax import lax
from jax.sharding import PartitionSpec as P

D = 2048
NOPE = 128
VDIM = 128
QK = 192
TOPK = 2
SEQS = 4
epsilon = 1e-06
rotary_base = 10000.0
lowest = -1e30


def rotate(values, positions):
    halfway = values.shape[-1] // 2
    inverse = rotary_base ** (-jnp.arange(halfway, dtype=jnp.float32) / halfway)
    angles = positions.astype(jnp.float32)[:, None] * inverse[None, :]
    angles = angles.reshape((angles.shape[0],) + (1,) * (values.ndim - 2) + (halfway,))
    cosine_values = jnp.cos(angles)
    sine_values = jnp.sin(angles)
    first_half = values[..., :halfway]
    second_half = values[..., halfway:]
    return jnp.concatenate(
        [
            first_half * cosine_values - second_half * sine_values,
            second_half * cosine_values + first_half * sine_values,
        ],
        axis=-1,
    )


def rms_scale(values, gain_values):
    return (
        values
        * lax.rsqrt(jnp.mean(values * values, axis=-1, keepdims=True) + epsilon)
        * gain_values
    )


def expand(latent_rows, latent_gain, key_up, value_up):
    normed = rms_scale(latent_rows.astype(jnp.float32), latent_gain).astype(jnp.bfloat16)
    keys_nope = jnp.dot(normed, key_up, preferred_element_type=jnp.float32).astype(jnp.bfloat16)
    values = jnp.dot(normed, value_up, preferred_element_type=jnp.float32).astype(jnp.bfloat16)
    lead = latent_rows.shape[:2]
    return (
        keys_nope.reshape(lead + (key_up.shape[1] // NOPE, NOPE)),
        values.reshape(lead + (value_up.shape[1] // VDIM, VDIM)),
    )


def absorb(carried, query_nope, query_rot, key_nope, value_rows, key_rot):
    running, totals, accumulated = carried
    scores = jnp.einsum("qshd,kshd->qshk", query_nope, key_nope, preferred_element_type=jnp.float32)
    scores = scores + jnp.einsum(
        "qshd,ksd->qshk", query_rot, key_rot, preferred_element_type=jnp.float32
    )
    scores = scores * QK ** (-0.5)
    highest = jnp.maximum(running, jnp.max(scores, axis=-1))
    weights = jnp.exp(scores - highest[..., None])
    totals = jnp.sum(weights, axis=-1)
    accumulated = jnp.einsum(
        "qshk,kshd->qshd",
        weights.astype(jnp.bfloat16),
        value_rows,
        preferred_element_type=jnp.float32,
    )
    return (highest, totals, accumulated)


def slots(chosen, row_count, experts_total):
    capacity = max(2, 3 * row_count * TOPK // (2 * experts_total))
    capacity = -(-capacity // 8) * 8
    one_hot = (chosen[:, None] == jnp.arange(experts_total, dtype=jnp.int32)[None, :]).astype(
        jnp.bfloat16
    )
    order = jnp.arange(chosen.shape[0])
    earlier = (order[:, None] > order[None, :]).astype(jnp.bfloat16)
    before = jnp.dot(earlier, one_hot, preferred_element_type=jnp.float32)
    slot_index = jnp.sum(before * one_hot.astype(jnp.float32), axis=-1).astype(jnp.int32)
    return (capacity, chosen * capacity + slot_index)


def whole_out_weight(out_weight):
    pieces = lax.axis_size("sp")
    depth = out_weight.shape[0] // pieces
    own = lax.dynamic_slice_in_dim(out_weight, lax.axis_index("sp") * depth, depth, axis=0)
    return lax.all_gather(own, ("tp", "sp"), axis=0, tiled=True)


def shards(
    residual,
    query,
    latent,
    rope_key,
    latent_gain,
    key_up,
    value_up,
    out_weight,
    norm_gain,
    group_prob,
    pair_logits,
    routes,
    w_gate,
    w_up,
    w_down,
):
    positions_here = query.shape[0]
    heads_here = key_up.shape[1] // NOPE
    own_positions = lax.axis_index("sp") * positions_here + jnp.arange(
        positions_here, dtype=jnp.int32
    )
    split_query = query.reshape(positions_here, SEQS, heads_here, QK)
    query_nope = split_query[..., :NOPE]
    query_rot = rotate(split_query[..., NOPE:].astype(jnp.float32), own_positions).astype(
        jnp.bfloat16
    )
    key_rot = rotate(rope_key.astype(jnp.float32), own_positions).astype(jnp.bfloat16)
    initial = (
        jnp.full((positions_here, SEQS, heads_here), lowest, jnp.float32),
        jnp.zeros((positions_here, SEQS, heads_here), jnp.float32),
        jnp.zeros((positions_here, SEQS, heads_here, VDIM), jnp.float32),
    )
    key_nope, value_rows = expand(
        lax.all_gather(latent, "sp", axis=0, tiled=True), latent_gain, key_up, value_up
    )
    finished = absorb(
        initial,
        query_nope,
        query_rot,
        key_nope,
        value_rows,
        lax.all_gather(key_rot, "sp", axis=0, tiled=True),
    )
    attended = (finished[2] / finished[1][..., None]).astype(jnp.bfloat16)
    attended = attended.reshape(positions_here, SEQS, heads_here * VDIM)
    by_token = lax.all_to_all(attended, "tp", split_axis=0, concat_axis=2, tiled=True)
    row_count = by_token.shape[0] * SEQS
    mixed_heads = by_token.reshape(row_count, by_token.shape[2])
    projected = jnp.dot(
        mixed_heads, whole_out_weight(out_weight), preferred_element_type=jnp.float32
    )
    stream = (residual.reshape(row_count, D).astype(jnp.float32) + projected).astype(jnp.bfloat16)
    normed = rms_scale(stream.astype(jnp.float32), norm_gain).astype(jnp.bfloat16)
    mixing = jax.nn.softmax(pair_logits.reshape(row_count, TOPK), axis=-1) * group_prob.reshape(
        row_count, 1
    )
    experts_total = lax.axis_size("sp") * lax.axis_size("tp")
    capacity, target = slots(routes.reshape(row_count * TOPK), row_count, experts_total)
    spots = target.reshape(row_count, TOPK)
    places = jnp.arange(experts_total * capacity, dtype=jnp.int32)
    picked = spots[:, :, None] == places[None, None, :]
    pick_rows = jnp.any(picked, axis=1).astype(jnp.bfloat16)
    outgoing = lax.dot_general(
        pick_rows, normed, (((0,), (0,)), ((), ())), preferred_element_type=jnp.float32
    ).astype(jnp.bfloat16)
    outgoing = outgoing.reshape(experts_total, capacity, D)
    arrived = lax.all_to_all(outgoing, ("sp", "tp"), split_axis=0, concat_axis=0, tiled=True)
    flat_rows = arrived.reshape(-1, D)
    gate_pre = jnp.dot(flat_rows, w_gate[0], preferred_element_type=jnp.float32)
    upward = jnp.dot(flat_rows, w_up[0], preferred_element_type=jnp.float32)
    hidden = (jax.nn.silu(gate_pre) * upward).astype(jnp.bfloat16)
    served = (
        jnp.dot(hidden, w_down[0], preferred_element_type=jnp.float32)
        .astype(jnp.bfloat16)
        .reshape(arrived.shape)
    )
    returned = lax.all_to_all(served, ("sp", "tp"), split_axis=0, concat_axis=0, tiled=True)
    returned = returned.reshape(experts_total * capacity, D)
    combined = stream.astype(jnp.float32)
    for choice in range(TOPK):
        combined = combined + mixing[:, choice, None] * jnp.dot(
            picked[:, choice].astype(jnp.bfloat16), returned, preferred_element_type=jnp.float32
        )
    return combined.astype(jnp.bfloat16).reshape(residual.shape)


def solution(mesh):
    placed = (
        P(("sp", "tp"), "grp", None),
        P("sp", "grp", "tp"),
        P("sp", "grp", None),
        P("sp", "grp", None),
        P(),
        P(None, "tp"),
        P(None, "tp"),
        P("tp", None),
        P(),
        P(("sp", "tp"), "grp"),
        P(("sp", "tp"), "grp", None),
        P(("sp", "tp"), "grp", None),
        P(("sp", "tp"), None, None),
        P(("sp", "tp"), None, None),
        P(("sp", "tp"), None, None),
    )
    return jax.shard_map(
        shards, mesh=mesh, in_specs=placed, out_specs=P(("sp", "tp"), "grp", None), check_vma=False
    )
```

profile of v0, /device:TPU:0, one launch (start us, length us, event | category | flops | bytes accessed | tf_op | source)
XLA Modules:
  0.0 262.8 jit_solution(14248461183122850936)
XLA Ops:
  6.5 0.7 all-gather.3.cloned.1.call-update
  7.3 0.0 all-gather.5.cloned.1.call-start
  7.3 1.9 constant_dynamic-slice_fusion
  9.2 0.0 all-gather.5.cloned.1.call-update
  9.2 2.0 copy.68
  11.2 3.2 %reshape.201 = bf16[192,4,2,192]{3,2,0,1:T(2,128)(2,1)} reshape(bf16[192,4,384]{2,0,1:T(8,128)(2,1)} %copy.68) | data formatting | bytes 1179648 | tf_op jit(solution)/shard_map/reshape | solution.py:115
  14.4 1.3 slice.43
  15.7 1.0 copy.99
  16.6 1.9 convert_element_type.90
  18.5 1.8 copy.71
  20.3 1.0 convert_element_type.88
  21.3 0.8 multiply_cosine_fusion
  22.1 1.5 copy.73
  23.6 1.5 copy.72
  25.1 1.3 subtract_convert_fusion
  26.5 0.3 pad_maximum_fusion
  26.8 0.0 copy-start.16
  26.8 14.9 %all_gather.10 = bf16[768,4,64]{2,1,0:T(4,128)(2,1)} all-gather(bf16[192,4,64]{2,1,0:T(4,128)(2,1)S(1)} %pad_maximum_fusion), channel_id=1, replica_groups=mesh['grp'=2,'sp'=4,'tp'=4] {'sp'}, dimensions={0}, use_global_device_ids=true | all-gather | bytes 491520 | tf_op jit(solution)/shard_map/all_gather | solution.py:135
  41.7 0.1 subtract_convert_fusion.1
  41.8 2.6 all-gather.3.cloned.1.call-done
  44.4 3.0 %fusion = f32[768,4]{0,1:T(4,128)S(1)} fusion(bf16[768,4,512]{2,1,0:T(4,128)(2,1)} %all-gather.3.cloned.1.call-done), kind=kLoop, calls=%fused_computation.2 | loop fusion | flops 4715520 | bytes 3158016 | tf_op jit(solution)/shard_map/reduce_sum | solution.py:38
  47.4 3.2 %fusion.26 = bf16[768,4,256]{0,2,1:T(8,128)(2,1)S(1)} fusion(f32[512]{0:T(512)S(1)} %copy-done.16, f32[768,4]{0,1:T(4,128)S(1)} %add_rsqrt_fusion, bf16[768,4,512]{2,1,0:T(4,128)(2,1)S(1)} %copy-done.2, bf16[512,256]{1,0:T(8,128)(2,1)} %param.20), kind=kOutput, calls=%fused_computation.31 | convolution fusion | flops 812384256 | bytes 4995072 | tf_op jit(solution)/shard_map/dot_general | solution.py:45
  50.6 0.8 fusion.46
  51.3 0.4 copy-done.3
  51.7 1.0 fusion.59
  52.7 1.3 fusion.4
  54.0 2.2 fusion.23
  56.3 1.2 fusion.38
  57.4 0.0 copy-start.11
  57.4 0.4 copy.96
  57.9 1.0 reshape.214
  58.9 4.6 %all-to-all-start = ((bf16[192,4,256]{2,1,0:T(4,128)(2,1)}), bf16[192,4,256]{2,1,0:T(4,128)(2,1)S(1)}, u32[]{:S(2)}, u32[]{:S(2)}) async-start(bf16[192,4,256]{2,1,0:T(4,128)(2,1)} %reshape.214), calls=%async_computation | async-start | bytes 786432 | tf_op jit(solution)/shard_map/all_to_all | solution.py:139
  63.5 2.5 reshape.210
  66.0 0.8 copy.85
  66.7 0.7 copy.84
  67.4 0.9 mul.224
  68.3 1.0 eq.28
  69.4 0.2 fusion.34
  69.6 0.8 convert_element_type.98
  70.4 1.0 copy.86
  71.4 1.7 iota_compare_fusion
  73.0 3.5 %all-to-all-done = bf16[192,4,256]{2,1,0:T(4,128)(2,1)S(1)} async-done(((bf16[192,4,256]{2,1,0:T(4,128)(2,1)}), bf16[192,4,256]{2,1,0:T(4,128)(2,1)S(1)}, u32[]{:S(2)}, u32[]{:S(2)}) %all-to-all-start) | async-done | bytes 393248 | tf_op jit(solution)/shard_map/all_to_all | solution.py:139
  76.6 0.3 copy.79
  76.9 0.1 copy.100
  77.0 21.5 %all-gather.5.cloned.1.call-done = bf16[1024,2048]{1,0:T(8,128)(2,1)} async-done(((bf16[64,2048]{1,0:T(8,128)(2,1)}), bf16[1024,2048]{1,0:T(8,128)(2,1)}) %all-gather.5.cloned.1.call-update) | async-done | bytes 4194320 | tf_op jit(solution)/shard_map/all_gather | solution.py:90
  98.5 3.8 %multiply_reduce_fusion = (f32[192]{0:T(256)S(1)}, f32[192,2048]{1,0:T(8,128)S(1)}) fusion(f32[192,2048]{1,0:T(8,128)} %reshape.210, bf16[192,1024]{1,0:T(8,128)(2,1)S(1)} %bitcast.72, bf16[1024,2048]{1,0:T(8,128)(2,1)} %all-gather.5.cloned.1.call-done), kind=kOutput, calls=%fused_computation.33 | convolution fusion | flops 807272256 | bytes 7734016 | tf_op jit(solution)/shard_map/dot_general | solution.py:142
  102.3 1.0 convolution_convert_fusion.1
  103.3 63.9 %all_to_all.25 = bf16[16,40,2048]{2,1,0:T(8,128)(2,1)S(1)} all-to-all(bf16[16,40,2048]{2,1,0:T(8,128)(2,1)S(1)} %bitcast.66), channel_id=1, replica_groups=mesh['grp'=2,'sp'=4,'tp'=4] {'sp','tp'}, dimensions={0} | all-to-all | bytes 5242880 | tf_op jit(solution)/shard_map/all_to_all | solution.py:160
  167.2 1.5 copy-done.4
  168.7 3.5 %fusion.9 = f32[640,768]{1,0:T(8,128)} fusion(bf16[640,2048]{1,0:T(8,128)(2,1)S(1)} %bitcast.70, bf16[1,2048,768]{2,1,0:T(8,128)(2,1)S(1)} %copy-done.14), kind=kOutput, calls=%fused_computation.15 | convolution fusion | flops 2013265920 | bytes 7733248 | tf_op jit(solution)/shard_map/dot_general | solution.py:162
  172.2 9.7 %convolution_convert_fusion = bf16[640,2048]{1,0:T(8,128)(2,1)} fusion(bf16[1,768,2048]{2,1,0:T(8,128)(2,1)S(1)} %copy-done, f32[640,768]{1,0:T(8,128)} %fusion.9, bf16[640,2048]{1,0:T(8,128)(2,1)} %bitcast.71, bf16[1,2048,768]{2,1,0:T(8,128)(2,1)} %param.28), kind=kOutput, calls=%fused_computation.10 | convolution fusion | flops 4030791680 | bytes 13500416 | tf_op jit(solution)/shard_map/dot_general | solution.py:166
  181.9 4.6 %all-to-all-start.2 = ((bf16[16,40,2048]{2,1,0:T(8,128)(2,1)}), bf16[16,40,2048]{2,1,0:T(8,128)(2,1)}, u32[]{:S(2)}, u32[]{:S(2)}) async-start(bf16[16,40,2048]{2,1,0:T(8,128)(2,1)} %bitcast.69), calls=%async_computation.2 | async-start | bytes 5242880 | tf_op jit(solution)/shard_map/all_to_all | solution.py:170
  186.5 0.1 copy.80
  186.6 0.1 reshape.204
  186.7 0.1 copy.83
  186.8 0.1 mul.217
  187.0 0.1 copy.81
  187.1 0.1 copy.82
  187.2 0.1 div.43
  187.3 0.1 sub.33
  187.4 59.7 %all-to-all-done.2 = bf16[16,40,2048]{2,1,0:T(8,128)(2,1)} async-done(((bf16[16,40,2048]{2,1,0:T(8,128)(2,1)}), bf16[16,40,2048]{2,1,0:T(8,128)(2,1)}, u32[]{:S(2)}, u32[]{:S(2)}) %all-to-all-start.2) | async-done | bytes 2621472 | tf_op jit(solution)/shard_map/all_to_all | solution.py:170
  247.1 3.0 %fusion.12 = f32[192,2048]{1,0:T(8,128)S(1)} fusion(f32[192,2048]{1,0:T(8,128)} %copy-done.1, bf16[640,2048]{1,0:T(8,128)(2,1)} %bitcast.18, f32[192]{0:T(256)S(1)} %bitcast.75, pred[192,2,640]{2,0,1:T(32,128)(4,1)S(1)} %copy-done.6), kind=kOutput, calls=%fused_computation.21 | convolution fusion | flops 504102912 | bytes 5891072 | tf_op jit(solution)/shard_map/dot_general | solution.py:174
  250.1 3.5 %fusion.13 = bf16[192,2048]{1,0:T(8,128)(2,1)} fusion(f32[192,2048]{1,0:T(8,128)S(1)} %fusion.12, bf16[640,2048]{1,0:T(8,128)(2,1)} %bitcast.18, f32[192]{0:T(256)S(1)} %bitcast.76, pred[192,2,640]{2,0,1:T(32,128)(4,1)S(1)} %copy-done.6), kind=kOutput, calls=%fused_computation.22 | convolution fusion | flops 504496128 | bytes 5104640 | tf_op jit(solution)/shard_map/dot_general | solution.py:174
  253.6 2.4 reshape.209
  (45 shorter events, 0.2 us)
Async XLA Ops:
  6.5 165.7 %copy-start = (bf16[1,768,2048]{2,1,0:T(8,128)(2,1)S(1)}, bf16[1,768,2048]{2,1,0:T(8,128)(2,1)}, u32[]{:S(2)}) copy-start(bf16[1,768,2048]{2,1,0:T(8,128)(2,1)} %param.29) | copy-start | bytes 9437188
  6.5 37.8 %all-gather.3.cloned.1.call-start = ((), (), s32[]{:S(2)}) async-start(), calls=%async_computation.3 | async-start | bytes 3932160 | tf_op jit(solution)/shard_map/all_gather | solution.py:127
  7.3 91.2 %all-gather.5.cloned.1.call-start = ((), (), s32[]{:S(2)}) async-start(), calls=%async_computation.4 | async-start | bytes 4456448 | tf_op jit(solution)/shard_map/all_gather | solution.py:90
  25.1 16.6 %copy-start.5 = (f32[192,4,2,64]{0,3,2,1:T(8,128)S(1)}, f32[192,4,2,64]{0,3,2,1:T(8,128)}, u32[]{:S(2)}) copy-start(f32[192,4,2,64]{0,3,2,1:T(8,128)} %convert_element_type.90) | copy-start | bytes 1179652
  25.1 16.6 %copy-start.8 = (f32[192,32]{0,1:T(8,128)S(1)}, f32[192,32]{0,1:T(8,128)}, u32[]{:S(2)}) copy-start(f32[192,32]{0,1:T(8,128)} %get-tuple-element.13) | copy-start | bytes 73732
  25.1 16.6 %copy-start.9 = (f32[192,32]{0,1:T(8,128)S(1)}, f32[192,32]{0,1:T(8,128)}, u32[]{:S(2)}) copy-start(f32[192,32]{0,1:T(8,128)} %get-tuple-element.14) | copy-start | bytes 73732
  26.8 20.6 %copy-start.16 = (f32[512]{0:T(512)S(1)}, f32[512]{0:T(512)}, u32[]{:S(2)}) copy-start(f32[512]{0:T(512)} %param.19) | copy-start | bytes 6148
  44.4 3.0 %copy-start.2 = (bf16[768,4,512]{2,1,0:T(4,128)(2,1)S(1)}, bf16[768,4,512]{2,1,0:T(4,128)(2,1)}, u32[]{:S(2)}) copy-start(bf16[768,4,512]{2,1,0:T(4,128)(2,1)} %all-gather.3.cloned.1.call-done) | copy-start | bytes 9437188
  47.4 3.2 %slice-start = ((bf16[192,4,2,192]{3,2,0,1:T(2,128)(2,1)}), bf16[192,4,2,128]{3,2,0,1:T(2,128)(2,1)S(1)}, s32[]{:S(2)}) async-start(bf16[192,4,2,192]{3,2,0,1:T(2,128)(2,1)} %reshape.201), calls=%async_computation.5 | async-start | bytes 786432 | tf_op jit(solution)/shard_map/slice | solution.py:116
  50.6 1.1 copy-start.3
  52.7 1.3 copy-start.15
  57.4 8.5 %copy-start.11 = (s32[48,4,2]{0,2,1:T(2,128)S(1)}, s32[48,4,2]{0,2,1:T(2,128)}, u32[]{:S(2)}) copy-start(s32[48,4,2]{0,2,1:T(2,128)} %param.26) | copy-start | bytes 4612
  58.9 17.7 %all-to-all-start = ((bf16[192,4,256]{2,1,0:T(4,128)(2,1)}), bf16[192,4,256]{2,1,0:T(4,128)(2,1)S(1)}, u32[]{:S(2)}, u32[]{:S(2)}) async-start(bf16[192,4,256]{2,1,0:T(4,128)(2,1)} %reshape.214), calls=%async_computation | async-start | bytes 786432 | tf_op jit(solution)/shard_map/all_to_all | solution.py:139
  98.5 3.8 %copy-start.7 = (pred[192,640]{1,0:T(8,128)(4,1)S(1)}, pred[192,640]{1,0:T(8,128)(4,1)}, u32[]{:S(2)}) copy-start(pred[192,640]{1,0:T(8,128)(4,1)} %get-tuple-element.12) | copy-start | bytes 368644
  98.5 3.8 %copy-start.12 = (f32[2048]{0:T(1024)S(1)}, f32[2048]{0:T(1024)}, u32[]{:S(2)}) copy-start(f32[2048]{0:T(1024)} %param.23) | copy-start | bytes 24580
  102.3 64.9 %copy-start.1 = (f32[192,2048]{1,0:T(8,128)}, f32[192,2048]{1,0:T(8,128)S(1)}, u32[]{:S(2)}) copy-start(f32[192,2048]{1,0:T(8,128)S(1)} %get-tuple-element.18) | copy-start | bytes 4718596
  103.3 65.4 %copy-start.14 = (bf16[1,2048,768]{2,1,0:T(8,128)(2,1)S(1)}, bf16[1,2048,768]{2,1,0:T(8,128)(2,1)}, u32[]{:S(2)}) copy-start(bf16[1,2048,768]{2,1,0:T(8,128)(2,1)} %param.27) | copy-start | bytes 9437188
  167.2 1.5 copy-start.4
  181.9 4.6 %copy-start.10 = (f32[48,4,2]{0,2,1:T(2,128)S(1)}, f32[48,4,2]{0,2,1:T(2,128)}, u32[]{:S(2)}) copy-start(f32[48,4,2]{0,2,1:T(2,128)} %param.25) | copy-start | bytes 4612
  181.9 4.8 %copy-start.13 = (f32[48,4]{0,1:T(4,128)S(1)}, f32[48,4]{0,1:T(4,128)}, u32[]{:S(2)}) copy-start(f32[48,4]{0,1:T(4,128)} %param.24) | copy-start | bytes 2308
  181.9 65.2 %copy-start.6 = (pred[192,2,640]{2,0,1:T(32,128)(4,1)S(1)}, pred[192,2,640]{2,0,1:T(32,128)(4,1)}, u32[]{:S(2)}) copy-start(pred[192,2,640]{2,0,1:T(32,128)(4,1)} %get-tuple-element.11) | copy-start | bytes 737284
  181.9 65.2 %all-to-all-start.2 = ((bf16[16,40,2048]{2,1,0:T(8,128)(2,1)}), bf16[16,40,2048]{2,1,0:T(8,128)(2,1)}, u32[]{:S(2)}, u32[]{:S(2)}) async-start(bf16[16,40,2048]{2,1,0:T(8,128)(2,1)} %bitcast.69), calls=%async_computation.2 | async-start | bytes 5242880 | tf_op jit(solution)/shard_map/all_to_all | solution.py:170
Sparse Core Ops, SparseCore 0:
  8.9 35.4 all-gather.2
  46.5 51.8 all-gather.4
where the time goes:
time: 264 us; the launch traced here: 263 us
  waiting for transfers between devices  88 us (33%)
  blocking collectives  78.8 us (30%)
  matrix products  33 us (12%)
  local copies, waits for them, and re-layouts  28.6 us (11%)
  between operations  13.7 us (5%)
  other arithmetic  11.4 us (4%)
  starting transfers between devices  9.24 us (4%)
    all_to_all x1, blocking collectives, shards(): lax.all_to_all(outgoing, ('sp', 'tp'), split_axis=0, concat_axis=0, tiled...  63.9 us
    all_to_all x1, waiting for transfers between devices, shards(): lax.all_to_all(served, ('sp', 'tp'), split_axis=0, concat_axis=0, tiled=T...  59.7 us
    all_gather x1, waiting for transfers between devices, whole_out_weight(): return lax.all_gather(own, ('tp', 'sp'), axis=0, tiled=True)  21.5 us
    all_gather x1, blocking collectives, shards(): lax.all_gather(key_rot, 'sp', axis=0, tiled=True)  14.9 us
    dot_general x1, matrix products, shards(): jnp.dot(hidden, w_down[0], preferred_element_type=jnp.float32)  9.66 us
    unnamed x41, local copies, waits for them, and re-layouts  7.63 us
    dot_general x2, matrix products, shards(): jnp.dot(picked[:, choice].astype(jnp.bfloat16), returned, preferred_eleme...  6.52 us
  transfers between devices with their start and end apart: 4, of which 4 were waited for; matrix products, arithmetic and copies ran while one was open for 17% of the time, Pallas kernels for 0%

commit v1 on v0

--- a/solution.py
+++ b/solution.py
@@ -2,6 +2,7 @@
 import jax.numpy as jnp
 from jax import lax
 from jax.sharding import PartitionSpec as P
+from jax.lax import axis_index, axis_size, ppermute
 
 D = 2048
 NOPE = 128
@@ -157,7 +158,20 @@
         pick_rows, normed, (((0,), (0,)), ((), ())), preferred_element_type=jnp.float32
     ).astype(jnp.bfloat16)
     outgoing = outgoing.reshape(experts_total, capacity, D)
-    arrived = lax.all_to_all(outgoing, ("sp", "tp"), split_axis=0, concat_axis=0, tiled=True)
+    after, back = (axis_size(("sp", "tp")), axis_index(("sp", "tp")))
+    o_now = outgoing.shape[0] // after
+    all_rows = jnp.roll(outgoing, -back * o_now, axis=0)
+    known = lax.slice_in_dim(all_rows, 0, o_now, axis=0)
+    fields = [known]
+    for dev_i in range(1, after):
+        outer = lax.slice_in_dim(all_rows, dev_i * o_now, (dev_i + 1) * o_now, axis=0)
+        fields.append(
+            ppermute(
+                outer, axis_name=("sp", "tp"), perm=[(k, (k + dev_i) % after) for k in range(after)]
+            )
+        )
+    tmp = jnp.concatenate(fields[::-1], axis=0)
+    arrived = jnp.roll(tmp, shift=(back + 1) * fields[0].shape[0], axis=0)
     flat_rows = arrived.reshape(-1, D)
     gate_pre = jnp.dot(flat_rows, w_gate[0], preferred_element_type=jnp.float32)
     upward = jnp.dot(flat_rows, w_up[0], preferred_element_type=jnp.float32)

time: 264 us -> 266 us (level)
  blocking collectives: 78.8 us -> 14.9 us
  waiting for transfers between devices: 88 us -> 119 us
  starting transfers between devices: 9.24 us -> 38.7 us
  local copies, waits for them, and re-layouts: 28.6 us -> 33.9 us
    all_to_all x1 -> x0, blocking collectives: 63.9 us -> none  [shards(): lax.all_to_all(outgoing, ('sp', 'tp'), split_axis=0, concat_axis=0, tiled...]
    ppermute x0 -> x15, starting transfers between devices: none -> 29.4 us  [shards(): ppermute(outer, axis_name=('sp', 'tp'), perm=[(k, (k + dev_i) % after) fo...]
    ppermute x0 -> x15, waiting for transfers between devices: none -> 29 us  [shards(): ppermute(outer, axis_name=('sp', 'tp'), perm=[(k, (k + dev_i) % after) fo...]
    unnamed x41 -> x62, local copies, waits for them, and re-layouts: 7.63 us -> 11.5 us
  transfers between devices with their start and end apart: 4 -> 19, of which waited for: 4 -> 8; matrix products, arithmetic and copies ran while one was open for 17% -> 16% of each run, Pallas kernels for 0% -> 0%
where the time goes in v1:
time: 266 us
  waiting for transfers between devices  119 us (45%)
  starting transfers between devices  38.7 us (15%)
  local copies, waits for them, and re-layouts  33.9 us (13%)
  matrix products  33 us (12%)
  blocking collectives  14.9 us (6%)
  between operations  13.9 us (5%)
  other arithmetic  11.7 us (4%)
    all_to_all x1, waiting for transfers between devices, shards(): lax.all_to_all(served, ('sp', 'tp'), split_axis=0, concat_axis=0, tiled=T...  59.7 us
    ppermute x15, starting transfers between devices, shards(): ppermute(outer, axis_name=('sp', 'tp'), perm=[(k, (k + dev_i) % after) fo...  29.4 us
    ppermute x15, waiting for transfers between devices, shards(): ppermute(outer, axis_name=('sp', 'tp'), perm=[(k, (k + dev_i) % after) fo...  29 us
    all_gather x1, waiting for transfers between devices, whole_out_weight(): return lax.all_gather(own, ('tp', 'sp'), axis=0, tiled=True)  21.5 us
    all_gather x1, blocking collectives, shards(): lax.all_gather(key_rot, 'sp', axis=0, tiled=True)  14.9 us
    unnamed x62, local copies, waits for them, and re-layouts  11.5 us
    dot_general x1, matrix products, shards(): jnp.dot(hidden, w_down[0], preferred_element_type=jnp.float32)  9.66 us
    dot_general x2, matrix products, shards(): jnp.dot(picked[:, choice].astype(jnp.bfloat16), returned, preferred_eleme...  6.51 us
  transfers between devices with their start and end apart: 19, of which 8 were waited for; matrix products, arithmetic and copies ran while one was open for 16% of the time, Pallas kernels for 0%

profile of v1, /device:TPU:0, one launch (start us, length us, event | category | flops | bytes accessed | tf_op | source)
XLA Modules:
  0.0 265.5 jit_solution(4109160225791945205)
XLA Ops:
  7.3 1.9 constant_dynamic-slice_fusion
  9.2 2.0 copy.68
  11.2 3.2 %reshape.201 = bf16[192,4,2,192]{3,2,0,1:T(2,128)(2,1)} reshape(bf16[192,4,384]{2,0,1:T(8,128)(2,1)} %copy.68) | data formatting | bytes 1179648 | tf_op jit(solution)/shard_map/reshape | solution.py:116
  14.4 2.0 slice.107
  16.7 0.7 copy.72
  18.2 0.9 copy.71
  19.1 1.0 convert_element_type.88
  20.0 1.9 copy.99
  21.9 1.0 convert_element_type.90
  22.9 1.3 subtract_convert_fusion
  24.5 14.9 %all_gather.10 = bf16[768,4,64]{2,1,0:T(4,128)(2,1)} all-gather(bf16[192,4,64]{2,1,0:T(4,128)(2,1)S(1)} %pad_maximum_fusion), channel_id=1, replica_groups=mesh['grp'=2,'sp'=4,'tp'=4] {'sp'}, dimensions={0}, use_global_device_ids=true | all-gather | bytes 491520 | tf_op jit(solution)/shard_map/all_gather | solution.py:136
  39.5 4.9 %all-gather.3.cloned.1.call-done = bf16[768,4,512]{2,1,0:T(4,128)(2,1)} async-done(((bf16[192,4,512]{2,1,0:T(4,128)(2,1)}), bf16[768,4,512]{2,1,0:T(4,128)(2,1)}) %all-gather.3.cloned.1.call-update) | async-done | bytes 3145744 | tf_op jit(solution)/shard_map/all_gather | solution.py:128
  44.4 3.0 %fusion = f32[768,4]{0,1:T(4,128)S(1)} fusion(bf16[768,4,512]{2,1,0:T(4,128)(2,1)} %all-gather.3.cloned.1.call-done), kind=kLoop, calls=%fused_computation.2 | loop fusion | flops 4715520 | bytes 3158016 | tf_op jit(solution)/shard_map/reduce_sum | solution.py:39
  47.4 3.2 %fusion.28 = bf16[768,4,256]{0,2,1:T(8,128)(2,1)S(1)} fusion(f32[512]{0:T(512)S(1)} %copy-done.19, f32[768,4]{0,1:T(4,128)S(1)} %add_rsqrt_fusion, bf16[768,4,512]{2,1,0:T(4,128)(2,1)S(1)} %copy-done.3, bf16[512,256]{1,0:T(8,128)(2,1)} %param.22), kind=kOutput, calls=%fused_computation.37 | convolution fusion | flops 812384256 | bytes 4995072 | tf_op jit(solution)/shard_map/dot_general | solution.py:46
  50.6 0.8 fusion.48
  51.8 1.0 fusion.62
  52.8 1.3 fusion.4
  54.1 2.2 fusion.25
  56.3 1.2 fusion.40
  57.9 1.0 reshape.214
  58.9 4.5 %all-to-all-start = ((bf16[192,4,256]{2,1,0:T(4,128)(2,1)}), bf16[192,4,256]{2,1,0:T(4,128)(2,1)S(1)}, u32[]{:S(2)}, u32[]{:S(2)}) async-start(bf16[192,4,256]{2,1,0:T(4,128)(2,1)} %reshape.214), calls=%async_computation | async-start | bytes 786432 | tf_op jit(solution)/shard_map/all_to_all | solution.py:140
  63.5 2.5 reshape.210
  66.0 0.7 copy.85
  66.7 1.0 eq.30
  68.0 0.8 convert_element_type.98
  68.7 1.0 copy.86
  69.7 0.7 copy.84
  70.4 0.9 mul.227
  71.4 1.7 iota_compare_fusion
  73.0 3.6 %all-to-all-done = bf16[192,4,256]{2,1,0:T(4,128)(2,1)S(1)} async-done(((bf16[192,4,256]{2,1,0:T(4,128)(2,1)}), bf16[192,4,256]{2,1,0:T(4,128)(2,1)S(1)}, u32[]{:S(2)}, u32[]{:S(2)}) %all-to-all-start) | async-done | bytes 393248 | tf_op jit(solution)/shard_map/all_to_all | solution.py:140
  77.0 21.5 %all-gather.5.cloned.1.call-done = bf16[1024,2048]{1,0:T(8,128)(2,1)} async-done(((bf16[64,2048]{1,0:T(8,128)(2,1)}), bf16[1024,2048]{1,0:T(8,128)(2,1)}) %all-gather.5.cloned.1.call-update) | async-done | bytes 4194320 | tf_op jit(solution)/shard_map/all_gather | solution.py:91
  98.5 3.8 %multiply_reduce_fusion = (f32[192]{0:T(256)S(1)}, f32[192,2048]{1,0:T(8,128)S(1)}) fusion(f32[192,2048]{1,0:T(8,128)} %reshape.210, bf16[192,1024]{1,0:T(8,128)(2,1)S(1)} %bitcast.72, bf16[1024,2048]{1,0:T(8,128)(2,1)} %all-gather.5.cloned.1.call-done), kind=kOutput, calls=%fused_computation.39 | convolution fusion | flops 807272256 | bytes 7734016 | tf_op jit(solution)/shard_map/dot_general | solution.py:143
  102.3 1.2 copy-done.1
  103.5 1.0 convolution_convert_fusion.1
  104.5 1.0 fusion.12
  105.4 1.5 copy-done.2
  106.9 1.3 fusion.60
  108.3 1.7 collective-permute-start
  110.0 0.9 collective-permute-start.1
  110.8 1.0 collective-permute-start.2
  111.9 1.0 collective-permute-start.3
  112.9 3.1 %collective-permute-start.4 = (bf16[1,40,2048]{2,1,0:T(8,128)(2,1)}, bf16[1,40,2048]{2,1,0:T(8,128)(2,1)S(1)}, u32[]{:S(2)}, u32[]{:S(2)}) collective-permute-start(bf16[1,40,2048]{2,1,0:T(8,128)(2,1)} %get-tuple-element.16), channel_id=1, source_target_pairs={{0,11},{1,12},{2,13},{3,14},{4,15},{5,0},{6,1},{7,2},{8,3},{9,4},{... | collective-permute-start | bytes 491528 | tf_op jit(solution)/shard_map/ppermute | solution.py:169
  116.0 1.5 collective-permute-start.5
  117.5 0.9 constant_dynamic-update-slice_fusion.14
  118.4 12.2 %collective-permute-done.1 = bf16[1,40,2048]{2,1,0:T(8,128)(2,1)S(1)} collective-permute-done((bf16[1,40,2048]{2,1,0:T(8,128)(2,1)}, bf16[1,40,2048]{2,1,0:T(8,128)(2,1)S(1)}, u32[]{:S(2)}, u32[]{:S(2)}) %collective-permute-start.1) | collective-permute-done | bytes 163872 | tf_op jit(solution)/shard_map/ppermute | solution.py:169
  131.3 3.3 %collective-permute-start.8 = (bf16[1,40,2048]{2,1,0:T(8,128)(2,1)}, bf16[1,40,2048]{2,1,0:T(8,128)(2,1)S(1)}, u32[]{:S(2)}, u32[]{:S(2)}) collective-permute-start(bf16[1,40,2048]{2,1,0:T(8,128)(2,1)} %get-tuple-element.12), channel_id=1, source_target_pairs={{0,7},{1,8},{2,9},{3,10},{4,11},{5,12},{6,13},{7,14},{8,15},{9,0},... | collective-permute-start | bytes 491528 | tf_op jit(solution)/shard_map/ppermute | solution.py:169
  134.6 2.3 collective-permute-start.9
  136.9 2.8 %collective-permute-done.5 = bf16[1,40,2048]{2,1,0:T(8,128)(2,1)S(1)} collective-permute-done((bf16[1,40,2048]{2,1,0:T(8,128)(2,1)}, bf16[1,40,2048]{2,1,0:T(8,128)(2,1)S(1)}, u32[]{:S(2)}, u32[]{:S(2)}) %collective-permute-start.5) | collective-permute-done | bytes 163872 | tf_op jit(solution)/shard_map/ppermute | solution.py:169
  139.7 3.9 %collective-permute-start.10 = (bf16[1,40,2048]{2,1,0:T(8,128)(2,1)}, bf16[1,40,2048]{2,1,0:T(8,128)(2,1)S(1)}, u32[]{:S(2)}, u32[]{:S(2)}) collective-permute-start(bf16[1,40,2048]{2,1,0:T(8,128)(2,1)} %get-tuple-element.10), channel_id=1, source_target_pairs={{0,5},{1,6},{2,7},{3,8},{4,9},{5,10},{6,11},{7,12},{8,13},{9,14},{... | collective-permute-start | bytes 491528 | tf_op jit(solution)/shard_map/ppermute | solution.py:169
  144.1 2.9 %collective-permute-start.12 = (bf16[1,40,2048]{2,1,0:T(8,128)(2,1)}, bf16[1,40,2048]{2,1,0:T(8,128)(2,1)S(1)}, u32[]{:S(2)}, u32[]{:S(2)}) collective-permute-start(bf16[1,40,2048]{2,1,0:T(8,128)(2,1)} %get-tuple-element.8), channel_id=1, source_target_pairs={{0,3},{1,4},{2,5},{3,6},{4,7},{5,8},{6,9},{7,10},{8,11},{9,12},{10... | collective-permute-start | bytes 491528 | tf_op jit(solution)/shard_map/ppermute | solution.py:169
  147.0 3.8 %collective-permute-start.13 = (bf16[1,40,2048]{2,1,0:T(8,128)(2,1)S(1)}, bf16[1,40,2048]{2,1,0:T(8,128)(2,1)S(1)}, u32[]{:S(2)}, u32[]{:S(2)}) collective-permute-start(bf16[1,40,2048]{2,1,0:T(8,128)(2,1)S(1)} %get-tuple-element.7), channel_id=1, source_target_pairs={{0,2},{1,3},{2,4},{3,5},{4,6},{5,7},{6,8},{7,9},{8,10},{9,11},{10,... | collective-permute-start | bytes 491528 | tf_op jit(solution)/shard_map/ppermute | solution.py:169
  150.9 4.4 %collective-permute-done.9 = bf16[1,40,2048]{2,1,0:T(8,128)(2,1)S(1)} collective-permute-done((bf16[1,40,2048]{2,1,0:T(8,128)(2,1)}, bf16[1,40,2048]{2,1,0:T(8,128)(2,1)S(1)}, u32[]{:S(2)}, u32[]{:S(2)}) %collective-permute-start.9) | collective-permute-done | bytes 163872 | tf_op jit(solution)/shard_map/ppermute | solution.py:169
  155.3 2.9 %collective-permute-start.14 = (bf16[1,40,2048]{2,1,0:T(8,128)(2,1)S(1)}, bf16[1,40,2048]{2,1,0:T(8,128)(2,1)S(1)}, u32[]{:S(2)}, u32[]{:S(2)}) collective-permute-start(bf16[1,40,2048]{2,1,0:T(8,128)(2,1)S(1)} %get-tuple-element.6), channel_id=1, source_target_pairs={{0,1},{1,2},{2,3},{3,4},{4,5},{5,6},{6,7},{7,8},{8,9},{9,10},{10,1... | collective-permute-start | bytes 491528 | tf_op jit(solution)/shard_map/ppermute | solution.py:169
  158.3 9.6 %collective-permute-done.13 = bf16[1,40,2048]{2,1,0:T(8,128)(2,1)S(1)} collective-permute-done((bf16[1,40,2048]{2,1,0:T(8,128)(2,1)S(1)}, bf16[1,40,2048]{2,1,0:T(8,128)(2,1)S(1)}, u32[]{:S(2)}, u32[]{:S(2)}) %collective-permute-start.13) | collective-permute-done | bytes 163872 | tf_op jit(solution)/shard_map/ppermute | solution.py:169
  167.9 0.9 slice_dynamic-update-slice_fusion
  168.9 1.0 fusion.11
  169.8 1.5 copy-done.5
  171.3 3.5 %fusion.9 = f32[640,768]{1,0:T(8,128)} fusion(bf16[640,2048]{1,0:T(8,128)(2,1)S(1)} %bitcast.70, bf16[1,2048,768]{2,1,0:T(8,128)(2,1)S(1)} %copy-done.17), kind=kOutput, calls=%fused_computation.19 | convolution fusion | flops 2013265920 | bytes 7733248 | tf_op jit(solution)/shard_map/dot_general | solution.py:176
  174.8 9.7 %convolution_convert_fusion = bf16[640,2048]{1,0:T(8,128)(2,1)} fusion(bf16[1,768,2048]{2,1,0:T(8,128)(2,1)S(1)} %copy-done, f32[640,768]{1,0:T(8,128)} %fusion.9, bf16[640,2048]{1,0:T(8,128)(2,1)} %bitcast.71, bf16[1,2048,768]{2,1,0:T(8,128)(2,1)} %param.30), kind=kOutput, calls=%fused_computation.14 | convolution fusion | flops 4030791680 | bytes 13500416 | tf_op jit(solution)/shard_map/dot_general | solution.py:180
  184.5 4.6 %all-to-all-start.1 = ((bf16[16,40,2048]{2,1,0:T(8,128)(2,1)}), bf16[16,40,2048]{2,1,0:T(8,128)(2,1)}, u32[]{:S(2)}, u32[]{:S(2)}) async-start(bf16[16,40,2048]{2,1,0:T(8,128)(2,1)} %bitcast.69), calls=%async_computation.1 | async-start | bytes 5242880 | tf_op jit(solution)/shard_map/all_to_all | solution.py:184
  190.1 59.7 %all-to-all-done.1 = bf16[16,40,2048]{2,1,0:T(8,128)(2,1)} async-done(((bf16[16,40,2048]{2,1,0:T(8,128)(2,1)}), bf16[16,40,2048]{2,1,0:T(8,128)(2,1)}, u32[]{:S(2)}, u32[]{:S(2)}) %all-to-all-start.1) | async-done | bytes 2621472 | tf_op jit(solution)/shard_map/all_to_all | solution.py:184
  249.8 3.0 %fusion.14 = f32[192,2048]{1,0:T(8,128)S(1)} fusion(f32[192,2048]{1,0:T(8,128)} %copy-done.1, bf16[640,2048]{1,0:T(8,128)(2,1)} %bitcast.18, f32[192]{0:T(256)S(1)} %bitcast.75, pred[192,2,640]{2,0,1:T(32,128)(4,1)S(1)} %copy-done.6), kind=kOutput, calls=%fused_computation.27 | convolution fusion | flops 504102912 | bytes 5891072 | tf_op jit(solution)/shard_map/dot_general | solution.py:188
  252.8 3.5 %fusion.15 = bf16[192,2048]{1,0:T(8,128)(2,1)} fusion(f32[192,2048]{1,0:T(8,128)S(1)} %fusion.14, bf16[640,2048]{1,0:T(8,128)(2,1)} %bitcast.18, f32[192]{0:T(256)S(1)} %bitcast.76, pred[192,2,640]{2,0,1:T(32,128)(4,1)S(1)} %copy-done.6), kind=kOutput, calls=%fused_computation.28 | convolution fusion | flops 504496128 | bytes 5104640 | tf_op jit(solution)/shard_map/dot_general | solution.py:188
  256.3 2.4 reshape.209
  (99 shorter events, 5.6 us)
Async XLA Ops:
  6.5 168.3 %copy-start = (bf16[1,768,2048]{2,1,0:T(8,128)(2,1)S(1)}, bf16[1,768,2048]{2,1,0:T(8,128)(2,1)}, u32[]{:S(2)}) copy-start(bf16[1,768,2048]{2,1,0:T(8,128)(2,1)} %param.31) | copy-start | bytes 9437188
  6.5 37.9 %all-gather.3.cloned.1.call-start = ((), (), s32[]{:S(2)}) async-start(), calls=%async_computation.2 | async-start | bytes 3932160 | tf_op jit(solution)/shard_map/all_gather | solution.py:128
  7.3 91.2 %all-gather.5.cloned.1.call-start = ((), (), s32[]{:S(2)}) async-start(), calls=%async_computation.3 | async-start | bytes 4456448 | tf_op jit(solution)/shard_map/all_gather | solution.py:91
  7.3 10.9 %copy-start.12 = (bf16[192,4,64]{0,2,1:T(8,128)(2,1)S(1)}, bf16[192,4,64]{0,2,1:T(8,128)(2,1)}, u32[]{:S(2)}) copy-start(bf16[192,4,64]{0,2,1:T(8,128)(2,1)} %param.20) | copy-start | bytes 294916
  16.7 1.5 copy-start.8
  16.7 1.5 copy-start.10
  21.9 17.5 %copy-start.9 = (f32[192,32]{0,1:T(8,128)S(1)}, f32[192,32]{0,1:T(8,128)}, u32[]{:S(2)}) copy-start(f32[192,32]{0,1:T(8,128)} %copy-done.8) | copy-start | bytes 73732
  21.9 17.5 %copy-start.11 = (f32[192,32]{0,1:T(8,128)S(1)}, f32[192,32]{0,1:T(8,128)}, u32[]{:S(2)}) copy-start(f32[192,32]{0,1:T(8,128)} %copy-done.10) | copy-start | bytes 73732
  24.5 22.9 %copy-start.19 = (f32[512]{0:T(512)S(1)}, f32[512]{0:T(512)}, u32[]{:S(2)}) copy-start(f32[512]{0:T(512)} %param.21) | copy-start | bytes 6148
  44.4 3.0 %copy-start.3 = (bf16[768,4,512]{2,1,0:T(4,128)(2,1)S(1)}, bf16[768,4,512]{2,1,0:T(4,128)(2,1)}, u32[]{:S(2)}) copy-start(bf16[768,4,512]{2,1,0:T(4,128)(2,1)} %all-gather.3.cloned.1.call-done) | copy-start | bytes 9437188
  47.4 3.2 %slice-start = ((bf16[192,4,2,192]{3,2,0,1:T(2,128)(2,1)}), bf16[192,4,2,128]{3,2,0,1:T(2,128)(2,1)S(1)}, s32[]{:S(2)}) async-start(bf16[192,4,2,192]{3,2,0,1:T(2,128)(2,1)} %reshape.201), calls=%async_computation.4 | async-start | bytes 786432 | tf_op jit(solution)/shard_map/slice | solution.py:117
  50.6 1.1 copy-start.4
  52.8 1.3 copy-start.18
  57.5 8.5 %copy-start.14 = (s32[48,4,2]{0,2,1:T(2,128)S(1)}, s32[48,4,2]{0,2,1:T(2,128)}, u32[]{:S(2)}) copy-start(s32[48,4,2]{0,2,1:T(2,128)} %param.28) | copy-start | bytes 4612
  58.9 17.7 %all-to-all-start = ((bf16[192,4,256]{2,1,0:T(4,128)(2,1)}), bf16[192,4,256]{2,1,0:T(4,128)(2,1)S(1)}, u32[]{:S(2)}, u32[]{:S(2)}) async-start(bf16[192,4,256]{2,1,0:T(4,128)(2,1)} %reshape.214), calls=%async_computation | async-start | bytes 786432 | tf_op jit(solution)/shard_map/all_to_all | solution.py:140
  98.5 5.0 %copy-start.7 = (pred[192,640]{1,0:T(8,128)(4,1)S(1)}, pred[192,640]{1,0:T(8,128)(4,1)}, u32[]{:S(2)}) copy-start(pred[192,640]{1,0:T(8,128)(4,1)} %get-tuple-element.28) | copy-start | bytes 368644
  98.5 5.0 %copy-start.15 = (f32[2048]{0:T(1024)S(1)}, f32[2048]{0:T(1024)}, u32[]{:S(2)}) copy-start(f32[2048]{0:T(1024)} %param.25) | copy-start | bytes 24580
  102.3 1.2 copy-start.1
  105.4 1.5 copy-start.2
  108.3 7.7 %collective-permute-start = (bf16[1,40,2048]{2,1,0:T(8,128)(2,1)}, bf16[1,40,2048]{2,1,0:T(8,128)(2,1)}, u32[]{:S(2)}, u32[]{:S(2)}) collective-permute-start(bf16[1,40,2048]{2,1,0:T(8,128)(2,1)} %get-tuple-element.20), channel_id=1, source_target_pairs={{0,15},{1,0},{2,1},{3,2},{4,3},{5,4},{6,5},{7,6},{8,7},{9,8},{10,9... | collective-permute-start | bytes 491528 | tf_op jit(solution)/shard_map/ppermute | solution.py:169
  110.0 20.6 %collective-permute-start.1 = (bf16[1,40,2048]{2,1,0:T(8,128)(2,1)}, bf16[1,40,2048]{2,1,0:T(8,128)(2,1)S(1)}, u32[]{:S(2)}, u32[]{:S(2)}) collective-permute-start(bf16[1,40,2048]{2,1,0:T(8,128)(2,1)} %get-tuple-element.19), channel_id=1, source_target_pairs={{0,14},{1,15},{2,0},{3,1},{4,2},{5,3},{6,4},{7,5},{8,6},{9,7},{10,... | collective-permute-start | bytes 491528 | tf_op jit(solution)/shard_map/ppermute | solution.py:169
  110.8 19.8 %collective-permute-start.2 = (bf16[1,40,2048]{2,1,0:T(8,128)(2,1)}, bf16[1,40,2048]{2,1,0:T(8,128)(2,1)S(1)}, u32[]{:S(2)}, u32[]{:S(2)}) collective-permute-start(bf16[1,40,2048]{2,1,0:T(8,128)(2,1)} %get-tuple-element.18), channel_id=1, source_target_pairs={{0,13},{1,14},{2,15},{3,0},{4,1},{5,2},{6,3},{7,4},{8,5},{9,6},{10... | collective-permute-start | bytes 491528 | tf_op jit(solution)/shard_map/ppermute | solution.py:169
  111.9 19.4 %collective-permute-start.3 = (bf16[1,40,2048]{2,1,0:T(8,128)(2,1)}, bf16[1,40,2048]{2,1,0:T(8,128)(2,1)S(1)}, u32[]{:S(2)}, u32[]{:S(2)}) collective-permute-start(bf16[1,40,2048]{2,1,0:T(8,128)(2,1)} %get-tuple-element.17), channel_id=1, source_target_pairs={{0,12},{1,13},{2,14},{3,15},{4,0},{5,1},{6,2},{7,3},{8,4},{9,5},{1... | collective-permute-start | bytes 491528 | tf_op jit(solution)/shard_map/ppermute | solution.py:169
  112.9 21.7 %collective-permute-start.4 = (bf16[1,40,2048]{2,1,0:T(8,128)(2,1)}, bf16[1,40,2048]{2,1,0:T(8,128)(2,1)S(1)}, u32[]{:S(2)}, u32[]{:S(2)}) collective-permute-start(bf16[1,40,2048]{2,1,0:T(8,128)(2,1)} %get-tuple-element.16), channel_id=1, source_target_pairs={{0,11},{1,12},{2,13},{3,14},{4,15},{5,0},{6,1},{7,2},{8,3},{9,4},{... | collective-permute-start | bytes 491528 | tf_op jit(solution)/shard_map/ppermute | solution.py:169
  116.0 23.7 %collective-permute-start.5 = (bf16[1,40,2048]{2,1,0:T(8,128)(2,1)}, bf16[1,40,2048]{2,1,0:T(8,128)(2,1)S(1)}, u32[]{:S(2)}, u32[]{:S(2)}) collective-permute-start(bf16[1,40,2048]{2,1,0:T(8,128)(2,1)} %get-tuple-element.15), channel_id=1, source_target_pairs={{0,10},{1,11},{2,12},{3,13},{4,14},{5,15},{6,0},{7,1},{8,2},{9,3},... | collective-permute-start | bytes 491528 | tf_op jit(solution)/shard_map/ppermute | solution.py:169
  130.6 13.0 %collective-permute-start.6 = (bf16[1,40,2048]{2,1,0:T(8,128)(2,1)}, bf16[1,40,2048]{2,1,0:T(8,128)(2,1)S(1)}, u32[]{:S(2)}, u32[]{:S(2)}) collective-permute-start(bf16[1,40,2048]{2,1,0:T(8,128)(2,1)} %get-tuple-element.14), channel_id=1, source_target_pairs={{0,9},{1,10},{2,11},{3,12},{4,13},{5,14},{6,15},{7,0},{8,1},{9,2},... | collective-permute-start | bytes 491528 | tf_op jit(solution)/shard_map/ppermute | solution.py:169
  130.6 13.5 %collective-permute-start.7 = (bf16[1,40,2048]{2,1,0:T(8,128)(2,1)}, bf16[1,40,2048]{2,1,0:T(8,128)(2,1)S(1)}, u32[]{:S(2)}, u32[]{:S(2)}) collective-permute-start(bf16[1,40,2048]{2,1,0:T(8,128)(2,1)} %get-tuple-element.13), channel_id=1, source_target_pairs={{0,8},{1,9},{2,10},{3,11},{4,12},{5,13},{6,14},{7,15},{8,0},{9,1},... | collective-permute-start | bytes 491528 | tf_op jit(solution)/shard_map/ppermute | solution.py:169
  131.3 15.7 %collective-permute-start.8 = (bf16[1,40,2048]{2,1,0:T(8,128)(2,1)}, bf16[1,40,2048]{2,1,0:T(8,128)(2,1)S(1)}, u32[]{:S(2)}, u32[]{:S(2)}) collective-permute-start(bf16[1,40,2048]{2,1,0:T(8,128)(2,1)} %get-tuple-element.12), channel_id=1, source_target_pairs={{0,7},{1,8},{2,9},{3,10},{4,11},{5,12},{6,13},{7,14},{8,15},{9,0},... | collective-permute-start | bytes 491528 | tf_op jit(solution)/shard_map/ppermute | solution.py:169
  134.6 20.7 %collective-permute-start.9 = (bf16[1,40,2048]{2,1,0:T(8,128)(2,1)}, bf16[1,40,2048]{2,1,0:T(8,128)(2,1)S(1)}, u32[]{:S(2)}, u32[]{:S(2)}) collective-permute-start(bf16[1,40,2048]{2,1,0:T(8,128)(2,1)} %get-tuple-element.11), channel_id=1, source_target_pairs={{0,6},{1,7},{2,8},{3,9},{4,10},{5,11},{6,12},{7,13},{8,14},{9,15},... | collective-permute-start | bytes 491528 | tf_op jit(solution)/shard_map/ppermute | solution.py:169
  139.7 18.5 %collective-permute-start.10 = (bf16[1,40,2048]{2,1,0:T(8,128)(2,1)}, bf16[1,40,2048]{2,1,0:T(8,128)(2,1)S(1)}, u32[]{:S(2)}, u32[]{:S(2)}) collective-permute-start(bf16[1,40,2048]{2,1,0:T(8,128)(2,1)} %get-tuple-element.10), channel_id=1, source_target_pairs={{0,5},{1,6},{2,7},{3,8},{4,9},{5,10},{6,11},{7,12},{8,13},{9,14},{... | collective-permute-start | bytes 491528 | tf_op jit(solution)/shard_map/ppermute | solution.py:169
  143.7 14.6 %collective-permute-start.11 = (bf16[1,40,2048]{2,1,0:T(8,128)(2,1)}, bf16[1,40,2048]{2,1,0:T(8,128)(2,1)S(1)}, u32[]{:S(2)}, u32[]{:S(2)}) collective-permute-start(bf16[1,40,2048]{2,1,0:T(8,128)(2,1)} %get-tuple-element.9), channel_id=1, source_target_pairs={{0,4},{1,5},{2,6},{3,7},{4,8},{5,9},{6,10},{7,11},{8,12},{9,13},{1... | collective-permute-start | bytes 491528 | tf_op jit(solution)/shard_map/ppermute | solution.py:169
  144.1 14.2 %collective-permute-start.12 = (bf16[1,40,2048]{2,1,0:T(8,128)(2,1)}, bf16[1,40,2048]{2,1,0:T(8,128)(2,1)S(1)}, u32[]{:S(2)}, u32[]{:S(2)}) collective-permute-start(bf16[1,40,2048]{2,1,0:T(8,128)(2,1)} %get-tuple-element.8), channel_id=1, source_target_pairs={{0,3},{1,4},{2,5},{3,6},{4,7},{5,8},{6,9},{7,10},{8,11},{9,12},{10... | collective-permute-start | bytes 491528 | tf_op jit(solution)/shard_map/ppermute | solution.py:169
  147.0 20.9 %collective-permute-start.13 = (bf16[1,40,2048]{2,1,0:T(8,128)(2,1)S(1)}, bf16[1,40,2048]{2,1,0:T(8,128)(2,1)S(1)}, u32[]{:S(2)}, u32[]{:S(2)}) collective-permute-start(bf16[1,40,2048]{2,1,0:T(8,128)(2,1)S(1)} %get-tuple-element.7), channel_id=1, source_target_pairs={{0,2},{1,3},{2,4},{3,5},{4,6},{5,7},{6,8},{7,9},{8,10},{9,11},{10,... | collective-permute-start | bytes 491528 | tf_op jit(solution)/shard_map/ppermute | solution.py:169
  155.3 12.6 %collective-permute-start.14 = (bf16[1,40,2048]{2,1,0:T(8,128)(2,1)S(1)}, bf16[1,40,2048]{2,1,0:T(8,128)(2,1)S(1)}, u32[]{:S(2)}, u32[]{:S(2)}) collective-permute-start(bf16[1,40,2048]{2,1,0:T(8,128)(2,1)S(1)} %get-tuple-element.6), channel_id=1, source_target_pairs={{0,1},{1,2},{2,3},{3,4},{4,5},{5,6},{6,7},{7,8},{8,9},{9,10},{10,1... | collective-permute-start | bytes 491528 | tf_op jit(solution)/shard_map/ppermute | solution.py:169
  168.9 2.5 copy-start.17
  169.8 1.5 copy-start.5
  184.5 4.7 %copy-start.13 = (f32[48,4,2]{0,2,1:T(2,128)S(1)}, f32[48,4,2]{0,2,1:T(2,128)}, u32[]{:S(2)}) copy-start(f32[48,4,2]{0,2,1:T(2,128)} %param.27) | copy-start | bytes 4612
  184.5 5.3 %copy-start.16 = (f32[48,4]{0,1:T(4,128)S(1)}, f32[48,4]{0,1:T(4,128)}, u32[]{:S(2)}) copy-start(f32[48,4]{0,1:T(4,128)} %param.26) | copy-start | bytes 2308
  184.5 65.3 %copy-start.6 = (pred[192,2,640]{2,0,1:T(32,128)(4,1)S(1)}, pred[192,2,640]{2,0,1:T(32,128)(4,1)}, u32[]{:S(2)}) copy-start(pred[192,2,640]{2,0,1:T(32,128)(4,1)} %get-tuple-element.27) | copy-start | bytes 737284
  184.5 65.3 %all-to-all-start.1 = ((bf16[16,40,2048]{2,1,0:T(8,128)(2,1)}), bf16[16,40,2048]{2,1,0:T(8,128)(2,1)}, u32[]{:S(2)}, u32[]{:S(2)}) async-start(bf16[16,40,2048]{2,1,0:T(8,128)(2,1)} %bitcast.69), calls=%async_computation.1 | async-start | bytes 5242880 | tf_op jit(solution)/shard_map/all_to_all | solution.py:184
Sparse Core Ops, SparseCore 0:
  8.9 35.5 all-gather.2
  46.6 51.8 all-gather.4
